TPU v7x, 128 devices: a whole 4x4x4 slice. The times are simulated.
128 devices in a mesh: sp: 16 (over z, y), tp: 8 (over x, core).
Axes of the slice: x: 4, y: 4, z: 4, core: 2. Of those that a mesh axis runs over, the one named last changes fastest.
Arguments:
- inputs: bfloat16 [16384, 2048], P('sp'), may hold values from -6 to 6
- norm_gain: float32 [3, 2048], replicated, may hold values from 0.1 to 1.9
- query_weight: bfloat16 [3, 2048, 1024], P(None, 'sp', 'tp'), may hold values from -64 to 64
- key_weight: bfloat16 [3, 2048, 512], P(None, 'sp', 'tp'), may hold values from -4 to 4
- value_weight: bfloat16 [3, 2048, 512], P(None, 'sp', 'tp'), may hold values from -0.125 to 0.125
- output_weight: bfloat16 [3, 2048, 1024], P(None, 'sp', 'tp'), may hold values from -0.1875 to 0.1875
- sink_logit: float32 [3, 16], P(None, 'tp'), may hold values from 2 to 7
- final_gain: float32 [2048], replicated, may hold values from 0.1 to 1.9
Outputs:
- result: float32 [16384, 2048], P(('sp', 'tp'))
All inputs are finite; a program needn't handle non-finite values.
Results may differ from a plain program's by a relative error of at most 0.015.
Values may be sent and summed in bfloat16 or wider, within the bound.
A program may use at most 64 MiB of HBM per device.

v0:
```python
import jax
import jax.numpy as jnp
from jax import lax
from jax.sharding import PartitionSpec as P

D = 2048
HEAD_DIM = 64
WINDOW = 128
LAYERS = 3
EPS = 1e-06


def sent_together(arrays, axis, dim, along):
    both = jnp.concatenate(arrays, axis=along)
    result, at, done = (lax.all_gather(both, axis, axis=dim, tiled=True), 0, [])
    for a in arrays:
        done.append(lax.slice_in_dim(result, at, at + a.shape[along], axis=along))
        at += a.shape[along]
    return tuple(done)


def extended_2(block, sides, width):
    for axis, dim in sides:
        count = lax.axis_size(axis)
        forward = [(i, i + 1) for i in range(count - 1)]
        backward = [(target, source) for source, target in forward]
        low = lax.ppermute(
            lax.slice_in_dim(block, block.shape[dim] - width, None, axis=dim), axis, forward
        )
        high = lax.ppermute(lax.slice_in_dim(block, 0, width, axis=dim), axis, backward)
        block = jnp.concatenate([low, block, high], axis=dim)
    return block


def norm_rows(values, gain):
    wide_values = values.astype(jnp.float32)
    inv_root = lax.rsqrt(jnp.mean(wide_values * wide_values, axis=-1, keepdims=True) + EPS)
    return wide_values * inv_root * gain


def rotate(values, places):
    half_dim = values.shape[-1] // 2
    inverse = 10000.0 ** (-jnp.arange(half_dim).astype(jnp.float32) / half_dim)
    angles = places[:, None] * inverse[None, :]
    cosine_table = jnp.cos(angles)[:, None, :]
    sine_table = jnp.sin(angles)[:, None, :]
    front_half = values[..., :half_dim]
    back_half = values[..., half_dim:]
    return jnp.concatenate(
        [
            front_half * cosine_table - back_half * sine_table,
            back_half * cosine_table + front_half * sine_table,
        ],
        axis=-1,
    )


def attend(queries, key_rows, value_rows, sink_row, allowed):
    scores = jnp.einsum(
        "qkgd,skd->kgqs", queries, key_rows, preferred_element_type=jnp.float32
    ) * queries.shape[-1] ** (-0.5)
    scores = jnp.where(allowed[None, None], scores, -jnp.inf)
    sink_col = sink_row[:, :, None]
    largest = jnp.maximum(jnp.max(scores, axis=-1), sink_col)
    powers = jnp.exp(scores - largest[..., None])
    denominator = jnp.sum(powers, axis=-1) + jnp.exp(sink_col - largest)
    weights = (powers / denominator[..., None]).astype(jnp.bfloat16)
    blended = jnp.einsum("kgqs,skd->qkgd", weights, value_rows, preferred_element_type=jnp.float32)
    return blended.astype(jnp.bfloat16)


def shards(
    inputs, norm_gain, query_weight, key_weight, value_weight, output_weight, sink_logit, final_gain
):
    tokens = inputs.shape[0]
    local_heads = query_weight.shape[2] // HEAD_DIM
    local_groups = key_weight.shape[2] // HEAD_DIM
    per_group = local_heads // local_groups
    kv_cols = local_groups * HEAD_DIM
    offset = lax.axis_index("sp") * tokens
    seq_total = tokens * lax.axis_size("sp")
    query_pos = offset + jnp.arange(tokens, dtype=jnp.int32)
    places = query_pos.astype(jnp.float32)
    key_pos = offset - WINDOW + jnp.arange(tokens + 2 * WINDOW, dtype=jnp.int32)
    allowed = (
        (jnp.abs(key_pos[None, :] - query_pos[:, None]) <= WINDOW)
        & (key_pos[None, :] >= 0)
        & (key_pos[None, :] < seq_total)
    )
    whole_query, whole_key, whole_value, whole_out = sent_together(
        (query_weight, key_weight, value_weight, output_weight), "sp", 1, 2
    )
    current = inputs
    final_rows = inputs
    for layer in range(LAYERS):
        normed = norm_rows(current, norm_gain[layer]).astype(jnp.bfloat16)
        query_raw = jnp.dot(normed, whole_query[layer], preferred_element_type=jnp.float32)
        key_raw = jnp.dot(normed, whole_key[layer], preferred_element_type=jnp.float32)
        value_raw = jnp.dot(normed, whole_value[layer], preferred_element_type=jnp.float32)
        out_weight = whole_out[layer]
        queries = rotate(
            (query_raw * float(D) ** (-0.5)).reshape(tokens, local_heads, HEAD_DIM), places
        ).astype(jnp.bfloat16)
        key_rot = rotate(
            (key_raw * float(D) ** (-0.5)).reshape(tokens, local_groups, HEAD_DIM), places
        ).astype(jnp.bfloat16)
        packed = jnp.concatenate(
            [key_rot.reshape(tokens, kv_cols), value_raw.astype(jnp.bfloat16)], axis=1
        )
        extended = extended_2(packed, (("sp", 0),), WINDOW)
        key_rows = extended[:, :kv_cols].reshape(-1, local_groups, HEAD_DIM)
        value_all = extended[:, kv_cols:].reshape(-1, local_groups, HEAD_DIM)
        sink_row = sink_logit[layer].reshape(local_groups, per_group)
        attended = attend(
            queries.reshape(tokens, local_groups, per_group, HEAD_DIM),
            key_rows,
            value_all,
            sink_row,
            allowed,
        )
        attended = attended.reshape(tokens, local_heads * HEAD_DIM)

        def project():
            return lax.dot_general(
                attended, out_weight, (((1,), (1,)), ((), ())), preferred_element_type=jnp.float32
            )

        if layer < LAYERS - 1:
            share_rows = lax.psum_scatter(project(), "tp", scatter_dimension=0, tiled=True).astype(
                jnp.bfloat16
            )
            current = lax.all_gather(share_rows, "tp", axis=0, tiled=True)
        else:
            final_rows = lax.psum_scatter(
                project().astype(jnp.bfloat16), "tp", scatter_dimension=0, tiled=True
            )
    return norm_rows(final_rows, final_gain)


def solution(mesh):
    in_specs = (
        P("sp", None),
        P(),
        P(None, "sp", "tp"),
        P(None, "sp", "tp"),
        P(None, "sp", "tp"),
        P(None, "sp", "tp"),
        P(None, "tp"),
        P(),
    )
    out_specs = P(("sp", "tp"), None)
    return jax.shard_map(shards, mesh=mesh, in_specs=in_specs, out_specs=out_specs, check_vma=False)
```

profile of v0, /device:TPU:0, one launch (start us, length us, event | category | flops | bytes accessed | tf_op | source)
XLA Modules:
  0.0 389.5 jit_solution(7353681811122570966)
XLA Ops:
  6.5 0.9 copy.9
  7.5 0.9 copy.10
  8.4 1.8 pad_maximum_fusion.3
  10.3 1.1 slice_reduce_fusion
  11.4 3.2 fusion.3
  14.7 0.5 multiply_cosine_fusion
  15.2 3.0 fusion.5
  18.2 2.2 fusion.22
  20.4 46.3 %all-gather.4.cloned.1.call-done = bf16[3,2048,384]{2,1,0:T(8,128)(2,1)} async-done(((bf16[3,128,384]{2,1,0:T(8,128)(2,1)}), bf16[3,2048,384]{2,1,0:T(8,128)(2,1)}) %all-gather.4.cloned.1.call-update) | async-done | bytes 4718608 | tf_op jit(solution)/shard_map/all_gather | solution.py:15
  66.8 3.9 fusion.34
  70.6 0.6 fusion.80
  71.2 2.5 convolution_convert_fusion.3
  73.7 3.4 collective-permute-start
  77.1 1.8 collective-permute-start.1
  78.9 2.6 convolution_multiply_fusion.2
  81.5 0.1 subtract_convert_fusion.2
  81.6 1.4 collective-permute-done.1
  83.0 2.2 fusion.12
  85.3 2.5 fusion
  87.8 0.1 exponential_add_fusion.2
  87.9 3.5 fusion.23
  91.4 5.6 %fusion.38 = f32[1024,2048]{1,0:T(8,128)} fusion(bf16[1024,128]{0,1:T(8,128)(2,1)S(1)} %bitcast.174, bf16[3,2048,384]{2,1,0:T(8,128)(2,1)} %all-gather.4.cloned.1.call-done), kind=kOutput, calls=%fused_computation.69 | convolution fusion | flops 536870912 | bytes 9175040 | tf_op jit(solution)/shard_map/dot_general | solution.py:124
  97.0 55.1 %reduce-scatter.4.cloned.1.call-done = f32[128,2048]{1,0:T(8,128)} async-done(((f32[1024,2048]{1,0:T(8,128)}), f32[128,2048]{1,0:T(8,128)}) %reduce-scatter.4.cloned.1.call-update) | async-done | bytes 1048592 | tf_op jit(solution)/shard_map/reduce_scatter | solution.py:129
  152.2 2.1 convert_element_type.126
  154.3 0.2 reduce-scatter.6.cloned.1.call-start
  154.5 31.6 %all-gather.6.cloned.1.call-done = bf16[1024,2048]{1,0:T(8,128)(2,1)} async-done(((bf16[128,2048]{1,0:T(8,128)(2,1)}), bf16[1024,2048]{1,0:T(8,128)(2,1)}) %all-gather.6.cloned.1.call-update) | async-done | bytes 4194320 | tf_op jit(solution)/shard_map/all_gather | solution.py:132
  186.1 3.2 fusion.6
  189.3 0.2 copy-done.3
  189.5 1.0 fusion.8
  190.6 2.5 fusion.33
  193.0 0.6 fusion.78
  193.6 2.5 convolution_convert_fusion.2
  196.1 3.4 collective-permute-start.2
  199.5 1.3 collective-permute-start.3
  200.8 2.6 convolution_multiply_fusion.1
  203.4 0.1 subtract_convert_fusion.1
  203.5 1.8 collective-permute-done.3
  205.4 2.2 fusion.13
  207.7 2.5 fusion.1
  210.2 0.1 exponential_add_fusion.1
  210.3 3.5 fusion.26
  213.8 5.6 %fusion.37 = f32[1024,2048]{1,0:T(8,128)} fusion(bf16[1024,128]{0,1:T(8,128)(2,1)S(1)} %bitcast.175, bf16[3,2048,384]{2,1,0:T(8,128)(2,1)} %all-gather.4.cloned.1.call-done), kind=kOutput, calls=%fused_computation.64 | convolution fusion | flops 536870912 | bytes 9175040 | tf_op jit(solution)/shard_map/dot_general | solution.py:124
  219.4 54.0 %reduce-scatter.6.cloned.1.call-done = f32[128,2048]{1,0:T(8,128)} async-done(((f32[1024,2048]{1,0:T(8,128)}), f32[128,2048]{1,0:T(8,128)}) %reduce-scatter.6.cloned.1.call-update) | async-done | bytes 1048592 | tf_op jit(solution)/shard_map/reduce_scatter | solution.py:129
  273.5 2.1 convert_element_type.134
  275.6 0.3 reduce-scatter.8.cloned.1.call-start
  275.8 31.5 %all-gather.8.cloned.1.call-done = bf16[1024,2048]{1,0:T(8,128)(2,1)} async-done(((bf16[128,2048]{1,0:T(8,128)(2,1)}), bf16[1024,2048]{1,0:T(8,128)(2,1)}) %all-gather.8.cloned.1.call-update) | async-done | bytes 4194320 | tf_op jit(solution)/shard_map/all_gather | solution.py:132
  307.4 3.2 fusion.9
  310.6 0.2 copy-done.2
  310.8 1.0 fusion.11
  311.8 2.4 fusion.32
  314.3 0.6 fusion.76
  314.8 2.5 convolution_convert_fusion.1
  317.4 3.4 collective-permute-start.4
  320.8 1.3 collective-permute-start.5
  322.1 2.6 convolution_multiply_fusion
  324.7 1.8 collective-permute-done.5
  326.6 2.2 fusion.14
  329.0 2.5 fusion.2
  331.4 0.1 exponential_add_fusion
  331.5 3.5 fusion.29
  335.1 4.3 %convolution_convert_fusion = bf16[1024,2048]{1,0:T(8,128)(2,1)} fusion(bf16[1024,128]{0,1:T(8,128)(2,1)S(1)} %bitcast.176, bf16[3,2048,384]{2,1,0:T(8,128)(2,1)} %all-gather.4.cloned.1.call-done), kind=kOutput, calls=%fused_computation.39 | convolution fusion | flops 538968064 | bytes 4980736 | tf_op jit(solution)/shard_map/dot_general | solution.py:124
  339.4 39.6 %reduce-scatter.8.cloned.1.call-done = bf16[128,2048]{1,0:T(8,128)(2,1)} async-done(((bf16[1024,2048]{1,0:T(8,128)(2,1)}), bf16[128,2048]{1,0:T(8,128)(2,1)}) %reduce-scatter.8.cloned.1.call-update) | async-done | bytes 524304 | tf_op jit(solution)/shard_map/reduce_scatter | solution.py:134
  379.0 1.2 fusion.35
  380.2 2.2 fusion.36
  (43 shorter events, 0.8 us)
Async XLA Ops:
  6.5 8.7 %copy-start.4 = (f32[3,2048]{1,0:T(4,128)S(1)}, f32[3,2048]{1,0:T(4,128)}, u32[]{:S(2)}) copy-start(f32[3,2048]{1,0:T(4,128)} %param.9) | copy-start | bytes 73732
  6.5 60.2 %all-gather.4.cloned.1.call-start = ((), (), s32[]{:S(2)}) async-start(), calls=%async_computation.3 | async-start | bytes 5013504 | tf_op jit(solution)/shard_map/all_gather | solution.py:15
  10.2 142.0 %reduce-scatter.4.cloned.1.call-start = ((), (), s32[]{:S(2)}) async-start(), calls=%async_computation.4 | async-start | bytes 9437184 | tf_op jit(solution)/shard_map/reduce_scatter | solution.py:129
  10.3 5.0 %copy-start.1 = (bf16[1024,2048]{1,0:T(8,128)(2,1)S(1)}, bf16[1024,2048]{1,0:T(8,128)(2,1)}, u32[]{:S(2)}) copy-start(bf16[1024,2048]{1,0:T(8,128)(2,1)} %param.8) | copy-start | bytes 12582916
  66.8 4.4 %copy-start = (bf16[1024,2048]{1,0:T(8,128)(2,1)S(1)}, bf16[1024,2048]{1,0:T(8,128)(2,1)}, u32[]{:S(2)}) copy-start(bf16[1024,2048]{1,0:T(8,128)(2,1)} %fusion.5) | copy-start | bytes 12582916
  73.7 7.8 %collective-permute-start = (bf16[128,128]{0,1:T(8,128)(2,1)S(1)}, bf16[128,128]{0,1:T(8,128)(2,1)S(1)}, u32[]{:S(2)}, u32[]{:S(2)}) collective-permute-start(bf16[128,128]{0,1:T(8,128)(2,1)S(1)} %get-tuple-element.24), channel_id=1, source_target_pairs={{0,8},{8,16},{16,24},{24,32},{32,40},{40,48},{48,56},{56,64},{64,7... | collective-permute-start | bytes 98312 | tf_op jit(solution)/shard_map/ppermute | solution.py:27
  77.1 5.8 %collective-permute-start.1 = (bf16[128,128]{0,1:T(8,128)(2,1)S(1)}, bf16[128,128]{0,1:T(8,128)(2,1)S(1)}, u32[]{:S(2)}, u32[]{:S(2)}) collective-permute-start(bf16[128,128]{0,1:T(8,128)(2,1)S(1)} %get-tuple-element.25), channel_id=1, source_target_pairs={{8,0},{16,8},{24,16},{32,24},{40,32},{48,40},{56,48},{64,56},{72,6... | collective-permute-start | bytes 98312 | tf_op jit(solution)/shard_map/ppermute | solution.py:30
  97.0 89.1 %all-gather.6.cloned.1.call-start = ((), (), s32[]{:S(2)}) async-start(), calls=%async_computation.5 | async-start | bytes 4718592 | tf_op jit(solution)/shard_map/all_gather | solution.py:132
  154.3 119.2 %reduce-scatter.6.cloned.1.call-start = ((), (), s32[]{:S(2)}) async-start(), calls=%async_computation.6 | async-start | bytes 9437184 | tf_op jit(solution)/shard_map/reduce_scatter | solution.py:129
  186.1 3.4 copy-start.3
  196.1 7.4 %collective-permute-start.2 = (bf16[128,128]{0,1:T(8,128)(2,1)S(1)}, bf16[128,128]{0,1:T(8,128)(2,1)S(1)}, u32[]{:S(2)}, u32[]{:S(2)}) collective-permute-start(bf16[128,128]{0,1:T(8,128)(2,1)S(1)} %get-tuple-element.22), channel_id=1, source_target_pairs={{0,8},{8,16},{16,24},{24,32},{32,40},{40,48},{48,56},{56,64},{64,7... | collective-permute-start | bytes 98312 | tf_op jit(solution)/shard_map/ppermute | solution.py:27
  199.5 5.8 %collective-permute-start.3 = (bf16[128,128]{0,1:T(8,128)(2,1)S(1)}, bf16[128,128]{0,1:T(8,128)(2,1)S(1)}, u32[]{:S(2)}, u32[]{:S(2)}) collective-permute-start(bf16[128,128]{0,1:T(8,128)(2,1)S(1)} %get-tuple-element.23), channel_id=1, source_target_pairs={{8,0},{16,8},{24,16},{32,24},{40,32},{48,40},{56,48},{64,56},{72,6... | collective-permute-start | bytes 98312 | tf_op jit(solution)/shard_map/ppermute | solution.py:30
  219.4 88.0 %all-gather.8.cloned.1.call-start = ((), (), s32[]{:S(2)}) async-start(), calls=%async_computation.7 | async-start | bytes 4718592 | tf_op jit(solution)/shard_map/all_gather | solution.py:132
  275.6 103.4 %reduce-scatter.8.cloned.1.call-start = ((), (), s32[]{:S(2)}) async-start(), calls=%async_computation.8 | async-start | bytes 4718592 | tf_op jit(solution)/shard_map/reduce_scatter | solution.py:134
  307.4 3.4 copy-start.2
  317.4 7.4 %collective-permute-start.4 = (bf16[128,128]{0,1:T(8,128)(2,1)S(1)}, bf16[128,128]{0,1:T(8,128)(2,1)S(1)}, u32[]{:S(2)}, u32[]{:S(2)}) collective-permute-start(bf16[128,128]{0,1:T(8,128)(2,1)S(1)} %get-tuple-element.20), channel_id=1, source_target_pairs={{0,8},{8,16},{16,24},{24,32},{32,40},{40,48},{48,56},{56,64},{64,7... | collective-permute-start | bytes 98312 | tf_op jit(solution)/shard_map/ppermute | solution.py:27
  320.8 5.8 %collective-permute-start.5 = (bf16[128,128]{0,1:T(8,128)(2,1)S(1)}, bf16[128,128]{0,1:T(8,128)(2,1)S(1)}, u32[]{:S(2)}, u32[]{:S(2)}) collective-permute-start(bf16[128,128]{0,1:T(8,128)(2,1)S(1)} %get-tuple-element.21), channel_id=1, source_target_pairs={{8,0},{16,8},{24,16},{32,24},{40,32},{48,40},{56,48},{64,56},{72,6... | collective-permute-start | bytes 98312 | tf_op jit(solution)/shard_map/ppermute | solution.py:30
  335.1 45.1 %copy-start.5 = (f32[2048]{0:T(1024)S(1)}, f32[2048]{0:T(1024)}, u32[]{:S(2)}) copy-start(f32[2048]{0:T(1024)} %param.15) | copy-start | bytes 24580
Sparse Core Ops, SparseCore 0:
  10.3 56.4 all-gather.3
  97.1 55.0 reduce-scatter.3
  154.4 31.6 all-gather.5
  219.5 53.9 reduce-scatter.5
  275.7 31.6 all-gather.7
  339.5 39.4 reduce-scatter.7
where the time goes:
time: 395 us; the launch traced here: 389 us
  waiting for transfers between devices  263 us (67%)
  matrix products  56.7 us (14%)
  other arithmetic  36.8 us (9%)
  starting transfers between devices  15.1 us (4%)
  between operations  14.1 us (4%)
    reduce_scatter x2, waiting for transfers between devices, shards(): lax.psum_scatter(project(), 'tp', scatter_dimension=0, tiled=True)  109 us
    all_gather x2, waiting for transfers between devices, shards(): current = lax.all_gather(share_rows, 'tp', axis=0, tiled=True)  63.1 us
    all_gather x1, waiting for transfers between devices, sent_together(): result, at, done = (lax.all_gather(both, axis, axis=dim, tiled=True), 0, [])  46.3 us
    reduce_scatter x1, waiting for transfers between devices, shards(): lax.psum_scatter(project().astype(jnp.bfloat16), 'tp', scatter_dimension=...  39.6 us
    dot_general x3, matrix products, project(): lax.dot_general(attended, out_weight, (((1,), (1,)), ((), ())), preferred...  15.4 us
    reduce_sum x4, other arithmetic, norm_rows(): jnp.mean(wide_values * wide_values, axis=-1, keepdims=True) + EPS  10.9 us
    dot_general x3, matrix products, attend(): jnp.einsum('kgqs,skd->qkgd', weights, value_rows, preferred_element_type=...  10.6 us
    ppermute x3, starting transfers between devices, extended_2(): lax.ppermute(lax.slice_in_dim(block, block.shape[dim] - width, None, axis...  10.2 us
  transfers between devices with their start and end apart: 12, of which 9 were waited for; matrix products, arithmetic and copies ran while one was open for 5% of the time, Pallas kernels for 0%

commit v1 on v0

--- a/solution.py
+++ b/solution.py
@@ -8,6 +8,24 @@
 WINDOW = 128
 LAYERS = 3
 EPS = 1e-06
+
+
+def ring_gather(value, axis, dim):
+    ways, here, step = (lax.axis_size(axis), lax.axis_index(axis), value.shape[dim])
+    lengths = [n * ways if d == dim else n for d, n in enumerate(value.shape)]
+    full = lax.dynamic_update_slice_in_dim(
+        jnp.zeros(lengths, value.dtype), value, here * step, axis=dim
+    )
+    going_up = going_down = value
+    for far in range(1, ways // 2 + 1):
+        going_up = lax.ppermute(going_up, axis, [(d, (d + 1) % ways) for d in range(ways)])
+        full = lax.dynamic_update_slice_in_dim(full, going_up, (here - far) % ways * step, axis=dim)
+        if 2 * far < ways:
+            going_down = lax.ppermute(going_down, axis, [(d, (d - 1) % ways) for d in range(ways)])
+            full = lax.dynamic_update_slice_in_dim(
+                full, going_down, (here + far) % ways * step, axis=dim
+            )
+    return full
 
 
 def sent_together(arrays, axis, dim, along):
@@ -129,7 +147,7 @@
             share_rows = lax.psum_scatter(project(), "tp", scatter_dimension=0, tiled=True).astype(
                 jnp.bfloat16
             )
-            current = lax.all_gather(share_rows, "tp", axis=0, tiled=True)
+            current = ring_gather(share_rows, "tp", 0)
         else:
             final_rows = lax.psum_scatter(
                 project().astype(jnp.bfloat16), "tp", scatter_dimension=0, tiled=True

time: 395 us -> 408 us (1.033)
  starting transfers between devices: 15.1 us -> 34.6 us
  waiting for transfers between devices: 263 us -> 250 us
  local copies, waits for them, and re-layouts: 3.38 us -> 13.9 us
    all_gather x2 -> x0, waiting for transfers between devices: 63.1 us -> none  [shards(): current = lax.all_gather(share_rows, 'tp', axis=0, tiled=True)]
    ppermute x0 -> x14, waiting for transfers between devices: none -> 54.3 us  [the longest x8 53.4 us: ring_gather(): lax.ppermute(going_up, axis, [(d, (d + 1) % ways) for d in range(ways)])]
    ppermute x0 -> x14, starting transfers between devices: none -> 17.9 us  [the longest x6 17.8 us: ring_gather(): lax.ppermute(going_down, axis, [(d, (d - 1) % ways) for d in range(ways)])]
    dynamic_update_slice x0 -> x14, local copies, waits for them, and re-layouts: none -> 7.23 us  [the longest x6 3.7 us: ring_gather(): lax.dynamic_update_slice_in_dim(full, going_down, (here + far) % ways * s...]
    convert_element_type x2 -> x0, other arithmetic: 4.17 us -> none  [shards(): lax.psum_scatter(project(), 'tp', scatter_dimension=0, tiled=True)]
  transfers between devices with their start and end apart: 12 -> 24, of which waited for: 9 -> 15; matrix products, arithmetic and copies ran while one was open for 5% -> 6% of each run, Pallas kernels for 0% -> 0%
where the time goes in v1:
time: 408 us; the launch traced here: 402 us
  waiting for transfers between devices  250 us (61%)
  matrix products  56.7 us (14%)
  starting transfers between devices  34.6 us (8%)
  other arithmetic  33.4 us (8%)
  local copies, waits for them, and re-layouts  13.9 us (3%)
  between operations  13.9 us (3%)
    reduce_scatter x2, waiting for transfers between devices, shards(): lax.psum_scatter(project(), 'tp', scatter_dimension=0, tiled=True)  108 us
    ppermute x8, waiting for transfers between devices, ring_gather(): lax.ppermute(going_up, axis, [(d, (d + 1) % ways) for d in range(ways)])  53.4 us
    all_gather x1, waiting for transfers between devices, sent_together(): result, at, done = (lax.all_gather(both, axis, axis=dim, tiled=True), 0, [])  46.3 us
    reduce_scatter x1, waiting for transfers between devices, shards(): lax.psum_scatter(project().astype(jnp.bfloat16), 'tp', scatter_dimension=...  38.5 us
    ppermute x6, starting transfers between devices, ring_gather(): lax.ppermute(going_down, axis, [(d, (d - 1) % ways) for d in range(ways)])  17.8 us
    dot_general x3, matrix products, project(): lax.dot_general(attended, out_weight, (((1,), (1,)), ((), ())), preferred...  15.4 us
    ppermute x3, starting transfers between devices, extended_2(): lax.ppermute(lax.slice_in_dim(block, block.shape[dim] - width, None, axis...  11.5 us
    dot_general x3, matrix products, attend(): jnp.einsum('kgqs,skd->qkgd', weights, value_rows, preferred_element_type=...  10.6 us
  transfers between devices with their start and end apart: 24, of which 15 were waited for; matrix products, arithmetic and copies ran while one was open for 6% of the time, Pallas kernels for 0%

profile of v1, /device:TPU:0, one launch (start us, length us, event | category | flops | bytes accessed | tf_op | source)
XLA Modules:
  0.0 402.4 jit_solution(4769108914522220408)
XLA Ops:
  6.5 0.9 copy.10
  7.5 0.9 copy.9
  8.4 1.8 pad_maximum_fusion.3
  10.3 1.1 slice_reduce_fusion
  11.4 3.2 fusion.3
  15.2 3.0 fusion.5
  18.2 2.2 fusion.22
  20.4 46.3 %all-gather.2.cloned.1.call-done = bf16[3,2048,384]{2,1,0:T(8,128)(2,1)} async-done(((bf16[3,128,384]{2,1,0:T(8,128)(2,1)}), bf16[3,2048,384]{2,1,0:T(8,128)(2,1)}) %all-gather.2.cloned.1.call-update) | async-done | bytes 4718608 | tf_op jit(solution)/shard_map/all_gather | solution.py:33
  66.8 3.9 fusion.34
  71.2 2.5 convolution_convert_fusion.3
  73.7 3.4 collective-permute-start
  77.1 1.6 collective-permute-start.1
  78.7 2.6 convolution_multiply_fusion.2
  81.4 1.6 collective-permute-done.1
  83.0 2.2 fusion.12
  85.3 2.5 fusion
  87.9 3.5 fusion.23
  91.4 5.6 %fusion.38 = f32[1024,2048]{1,0:T(8,128)} fusion(bf16[1024,128]{0,1:T(8,128)(2,1)S(1)} %bitcast.174, bf16[3,2048,384]{2,1,0:T(8,128)(2,1)} %all-gather.2.cloned.1.call-done), kind=kOutput, calls=%fused_computation.69 | convolution fusion | flops 536870912 | bytes 9175040 | tf_op jit(solution)/shard_map/dot_general | solution.py:142
  97.6 54.6 %reduce-scatter.4.cloned.1.call-done = f32[128,2048]{1,0:T(8,128)} async-done(((f32[1024,2048]{1,0:T(8,128)}), f32[128,2048]{1,0:T(8,128)}) %reduce-scatter.4.cloned.1.call-update) | async-done | bytes 1048592 | tf_op jit(solution)/shard_map/reduce_scatter | solution.py:147
  152.2 2.5 broadcast.326.clone
  154.7 0.9 constant_dynamic-update-slice_fusion.15
  155.6 3.0 collective-permute-start.3
  158.5 6.9 %collective-permute-done.2 = bf16[128,2048]{1,0:T(8,128)(2,1)S(1)} collective-permute-done((bf16[128,2048]{1,0:T(8,128)(2,1)S(1)}, bf16[128,2048]{1,0:T(8,128)(2,1)S(1)}, u32[]{:S(2)}, u32[]{:S(2)}) %collective-permute-start.2) | collective-permute-done | bytes 524320 | tf_op jit(solution)/shard_map/ppermute | solution.py:21
  165.4 3.1 collective-permute-start.5
  168.5 6.8 %collective-permute-done.4 = bf16[128,2048]{1,0:T(8,128)(2,1)S(1)} collective-permute-done((bf16[128,2048]{1,0:T(8,128)(2,1)S(1)}, bf16[128,2048]{1,0:T(8,128)(2,1)S(1)}, u32[]{:S(2)}, u32[]{:S(2)}) %collective-permute-start.4) | collective-permute-done | bytes 524320 | tf_op jit(solution)/shard_map/ppermute | solution.py:21
  176.0 1.9 constant_dynamic-update-slice_fusion.13
  177.9 3.0 collective-permute-start.7
  181.7 3.3 collective-permute-done.6
  186.7 0.9 collective-permute-done.7
  188.4 6.4 %collective-permute-done.8 = bf16[128,2048]{1,0:T(8,128)(2,1)S(1)} collective-permute-done((bf16[128,2048]{1,0:T(8,128)(2,1)S(1)}, bf16[128,2048]{1,0:T(8,128)(2,1)S(1)}, u32[]{:S(2)}, u32[]{:S(2)}) %collective-permute-start.8) | collective-permute-done | bytes 524320 | tf_op jit(solution)/shard_map/ppermute | solution.py:21
  195.7 3.1 fusion.6
  198.8 3.2 fusion.8
  202.0 2.5 fusion.33
  205.0 2.5 convolution_convert_fusion.2
  207.6 1.3 collective-permute-start.10
  208.9 4.7 %collective-permute-start.9 = (bf16[128,128]{0,1:T(8,128)(2,1)S(1)}, bf16[128,128]{0,1:T(8,128)(2,1)S(1)}, u32[]{:S(2)}, u32[]{:S(2)}) collective-permute-start(bf16[128,128]{0,1:T(8,128)(2,1)S(1)} %get-tuple-element.26), channel_id=1, source_target_pairs={{0,8},{8,16},{16,24},{24,32},{32,40},{40,48},{48,56},{56,64},{64,7... | collective-permute-start | bytes 98312 | tf_op jit(solution)/shard_map/ppermute | solution.py:45
  213.6 2.6 convolution_multiply_fusion.1
  216.3 2.2 fusion.13
  218.6 2.5 fusion.1
  221.2 3.5 fusion.26
  224.7 5.6 %fusion.37 = f32[1024,2048]{1,0:T(8,128)} fusion(bf16[1024,128]{0,1:T(8,128)(2,1)S(1)} %bitcast.175, bf16[3,2048,384]{2,1,0:T(8,128)(2,1)} %all-gather.2.cloned.1.call-done), kind=kOutput, calls=%fused_computation.64 | convolution fusion | flops 536870912 | bytes 9175040 | tf_op jit(solution)/shard_map/dot_general | solution.py:142
  230.6 53.0 %reduce-scatter.6.cloned.1.call-done = f32[128,2048]{1,0:T(8,128)} async-done(((f32[1024,2048]{1,0:T(8,128)}), f32[128,2048]{1,0:T(8,128)}) %reduce-scatter.6.cloned.1.call-update) | async-done | bytes 1048592 | tf_op jit(solution)/shard_map/reduce_scatter | solution.py:147
  284.9 2.9 collective-permute-start.12
  287.9 6.9 %collective-permute-done.11 = bf16[128,2048]{1,0:T(8,128)(2,1)S(1)} collective-permute-done((bf16[128,2048]{1,0:T(8,128)(2,1)S(1)}, bf16[128,2048]{1,0:T(8,128)(2,1)S(1)}, u32[]{:S(2)}, u32[]{:S(2)}) %collective-permute-start.11) | collective-permute-done | bytes 524320 | tf_op jit(solution)/shard_map/ppermute | solution.py:21
  294.7 3.0 collective-permute-start.14
  297.7 6.9 %collective-permute-done.13 = bf16[128,2048]{1,0:T(8,128)(2,1)S(1)} collective-permute-done((bf16[128,2048]{1,0:T(8,128)(2,1)S(1)}, bf16[128,2048]{1,0:T(8,128)(2,1)S(1)}, u32[]{:S(2)}, u32[]{:S(2)}) %collective-permute-start.13) | collective-permute-done | bytes 524320 | tf_op jit(solution)/shard_map/ppermute | solution.py:21
  304.7 3.0 collective-permute-start.16
  307.7 6.7 %collective-permute-done.15 = bf16[128,2048]{1,0:T(8,128)(2,1)S(1)} collective-permute-done((bf16[128,2048]{1,0:T(8,128)(2,1)S(1)}, bf16[128,2048]{1,0:T(8,128)(2,1)S(1)}, u32[]{:S(2)}, u32[]{:S(2)}) %collective-permute-start.15) | collective-permute-done | bytes 524320 | tf_op jit(solution)/shard_map/ppermute | solution.py:21
  314.6 9.6 %collective-permute-done.17 = bf16[128,2048]{1,0:T(8,128)(2,1)S(1)} collective-permute-done((bf16[128,2048]{1,0:T(8,128)(2,1)S(1)}, bf16[128,2048]{1,0:T(8,128)(2,1)S(1)}, u32[]{:S(2)}, u32[]{:S(2)}) %collective-permute-start.17) | collective-permute-done | bytes 524320 | tf_op jit(solution)/shard_map/ppermute | solution.py:21
  324.2 0.9 fusion.9
  325.1 1.0 fusion.11
  326.2 2.4 fusion.32
  329.2 2.5 convolution_convert_fusion.1
  331.7 3.4 collective-permute-start.18
  335.1 1.5 collective-permute-start.19
  336.7 2.6 convolution_multiply_fusion
  339.3 1.6 collective-permute-done.19
  341.0 2.2 fusion.14
  343.3 2.5 fusion.2
  345.9 3.5 fusion.29
  349.4 4.3 %convolution_convert_fusion = bf16[1024,2048]{1,0:T(8,128)(2,1)} fusion(bf16[1024,128]{0,1:T(8,128)(2,1)S(1)} %bitcast.176, bf16[3,2048,384]{2,1,0:T(8,128)(2,1)} %all-gather.2.cloned.1.call-done), kind=kOutput, calls=%fused_computation.39 | convolution fusion | flops 538968064 | bytes 4980736 | tf_op jit(solution)/shard_map/dot_general | solution.py:142
  353.7 38.5 %reduce-scatter.8.cloned.1.call-done = bf16[128,2048]{1,0:T(8,128)(2,1)} async-done(((bf16[1024,2048]{1,0:T(8,128)(2,1)}), bf16[128,2048]{1,0:T(8,128)(2,1)}) %reduce-scatter.8.cloned.1.call-update) | async-done | bytes 524304 | tf_op jit(solution)/shard_map/reduce_scatter | solution.py:152
  392.2 1.2 fusion.35
  393.4 2.2 fusion.36
  (81 shorter events, 10.8 us)
Async XLA Ops:
  6.5 8.7 %copy-start.4 = (f32[3,2048]{1,0:T(4,128)S(1)}, f32[3,2048]{1,0:T(4,128)}, u32[]{:S(2)}) copy-start(f32[3,2048]{1,0:T(4,128)} %param.9) | copy-start | bytes 73732
  6.5 60.2 %all-gather.2.cloned.1.call-start = ((), (), s32[]{:S(2)}) async-start(), calls=%async_computation.3 | async-start | bytes 5013504 | tf_op jit(solution)/shard_map/all_gather | solution.py:33
  10.2 142.0 %reduce-scatter.4.cloned.1.call-start = ((), (), s32[]{:S(2)}) async-start(), calls=%async_computation.4 | async-start | bytes 9437184 | tf_op jit(solution)/shard_map/reduce_scatter | solution.py:147
  10.3 5.0 %copy-start.1 = (bf16[1024,2048]{1,0:T(8,128)(2,1)S(1)}, bf16[1024,2048]{1,0:T(8,128)(2,1)}, u32[]{:S(2)}) copy-start(bf16[1024,2048]{1,0:T(8,128)(2,1)} %param.8) | copy-start | bytes 12582916
  66.8 4.4 %copy-start = (bf16[1024,2048]{1,0:T(8,128)(2,1)S(1)}, bf16[1024,2048]{1,0:T(8,128)(2,1)}, u32[]{:S(2)}) copy-start(bf16[1024,2048]{1,0:T(8,128)(2,1)} %fusion.5) | copy-start | bytes 12582916
  73.7 7.6 %collective-permute-start = (bf16[128,128]{0,1:T(8,128)(2,1)S(1)}, bf16[128,128]{0,1:T(8,128)(2,1)S(1)}, u32[]{:S(2)}, u32[]{:S(2)}) collective-permute-start(bf16[128,128]{0,1:T(8,128)(2,1)S(1)} %get-tuple-element.28), channel_id=1, source_target_pairs={{0,8},{8,16},{16,24},{24,32},{32,40},{40,48},{48,56},{56,64},{64,7... | collective-permute-start | bytes 98312 | tf_op jit(solution)/shard_map/ppermute | solution.py:45
  77.1 5.8 %collective-permute-start.1 = (bf16[128,128]{0,1:T(8,128)(2,1)S(1)}, bf16[128,128]{0,1:T(8,128)(2,1)S(1)}, u32[]{:S(2)}, u32[]{:S(2)}) collective-permute-start(bf16[128,128]{0,1:T(8,128)(2,1)S(1)} %get-tuple-element.29), channel_id=1, source_target_pairs={{8,0},{16,8},{24,16},{32,24},{40,32},{48,40},{56,48},{64,56},{72,6... | collective-permute-start | bytes 98312 | tf_op jit(solution)/shard_map/ppermute | solution.py:48
  97.0 186.6 %reduce-scatter.6.cloned.1.call-start = ((), (), s32[]{:S(2)}) async-start(), calls=%async_computation.5 | async-start | bytes 9437184 | tf_op jit(solution)/shard_map/reduce_scatter | solution.py:147
  152.2 2.5 copy-start.2
  155.6 9.8 %collective-permute-start.2 = (bf16[128,2048]{1,0:T(8,128)(2,1)S(1)}, bf16[128,2048]{1,0:T(8,128)(2,1)S(1)}, u32[]{:S(2)}, u32[]{:S(2)}) collective-permute-start(bf16[128,2048]{1,0:T(8,128)(2,1)S(1)} %get-tuple-element.11), channel_id=1, source_target_pairs={{0,1},{1,2},{2,3},{3,4},{4,5},{5,6},{6,7},{7,0},{8,9},{9,10},{10,1... | collective-permute-start | bytes 1572872 | tf_op jit(solution)/shard_map/ppermute | solution.py:21
  155.6 9.8 %collective-permute-start.3 = (bf16[128,2048]{1,0:T(8,128)(2,1)S(1)}, bf16[128,2048]{1,0:T(8,128)(2,1)}, u32[]{:S(2)}, u32[]{:S(2)}) collective-permute-start(bf16[128,2048]{1,0:T(8,128)(2,1)S(1)} %get-tuple-element.11), channel_id=1, source_target_pairs={{0,7},{1,0},{2,1},{3,2},{4,3},{5,4},{6,5},{7,6},{8,15},{9,8},{10,9... | collective-permute-start | bytes 1572872 | tf_op jit(solution)/shard_map/ppermute | solution.py:24
  165.4 9.8 %collective-permute-start.4 = (bf16[128,2048]{1,0:T(8,128)(2,1)S(1)}, bf16[128,2048]{1,0:T(8,128)(2,1)S(1)}, u32[]{:S(2)}, u32[]{:S(2)}) collective-permute-start(bf16[128,2048]{1,0:T(8,128)(2,1)S(1)} %collective-permute-done.2), channel_id=1, source_target_pairs={{0,1},{1,2},{2,3},{3,4},{4,5},{5,6},{6,7},{7,0},{8,9},{9,10},{10,1... | collective-permute-start | bytes 1572872 | tf_op jit(solution)/shard_map/ppermute | solution.py:21
  165.4 12.5 %collective-permute-start.5 = (bf16[128,2048]{1,0:T(8,128)(2,1)}, bf16[128,2048]{1,0:T(8,128)(2,1)S(1)}, u32[]{:S(2)}, u32[]{:S(2)}) collective-permute-start(bf16[128,2048]{1,0:T(8,128)(2,1)} %collective-permute-done.3), channel_id=1, source_target_pairs={{0,7},{1,0},{2,1},{3,2},{4,3},{5,4},{6,5},{7,6},{8,15},{9,8},{10,9... | collective-permute-start | bytes 1572872 | tf_op jit(solution)/shard_map/ppermute | solution.py:24
  175.2 9.8 %collective-permute-start.6 = (bf16[128,2048]{1,0:T(8,128)(2,1)S(1)}, bf16[128,2048]{1,0:T(8,128)(2,1)S(1)}, u32[]{:S(2)}, u32[]{:S(2)}) collective-permute-start(bf16[128,2048]{1,0:T(8,128)(2,1)S(1)} %collective-permute-done.4), channel_id=1, source_target_pairs={{0,1},{1,2},{2,3},{3,4},{4,5},{5,6},{6,7},{7,0},{8,9},{9,10},{10,1... | collective-permute-start | bytes 1572872 | tf_op jit(solution)/shard_map/ppermute | solution.py:21
  177.9 9.7 %collective-permute-start.7 = (bf16[128,2048]{1,0:T(8,128)(2,1)S(1)}, bf16[128,2048]{1,0:T(8,128)(2,1)S(1)}, u32[]{:S(2)}, u32[]{:S(2)}) collective-permute-start(bf16[128,2048]{1,0:T(8,128)(2,1)S(1)} %collective-permute-done.5), channel_id=1, source_target_pairs={{0,7},{1,0},{2,1},{3,2},{4,3},{5,4},{6,5},{7,6},{8,15},{9,8},{10,9... | collective-permute-start | bytes 1572872 | tf_op jit(solution)/shard_map/ppermute | solution.py:24
  185.0 9.8 %collective-permute-start.8 = (bf16[128,2048]{1,0:T(8,128)(2,1)S(1)}, bf16[128,2048]{1,0:T(8,128)(2,1)S(1)}, u32[]{:S(2)}, u32[]{:S(2)}) collective-permute-start(bf16[128,2048]{1,0:T(8,128)(2,1)S(1)} %collective-permute-done.6), channel_id=1, source_target_pairs={{0,1},{1,2},{2,3},{3,4},{4,5},{5,6},{6,7},{7,0},{8,9},{9,10},{10,1... | collective-permute-start | bytes 1572872 | tf_op jit(solution)/shard_map/ppermute | solution.py:21
  207.6 8.7 %collective-permute-start.10 = (bf16[128,128]{0,1:T(8,128)(2,1)S(1)}, bf16[128,128]{0,1:T(8,128)(2,1)S(1)}, u32[]{:S(2)}, u32[]{:S(2)}) collective-permute-start(bf16[128,128]{0,1:T(8,128)(2,1)S(1)} %get-tuple-element.27), channel_id=1, source_target_pairs={{8,0},{16,8},{24,16},{32,24},{40,32},{48,40},{56,48},{64,56},{72,6... | collective-permute-start | bytes 98312 | tf_op jit(solution)/shard_map/ppermute | solution.py:48
  208.9 7.4 %collective-permute-start.9 = (bf16[128,128]{0,1:T(8,128)(2,1)S(1)}, bf16[128,128]{0,1:T(8,128)(2,1)S(1)}, u32[]{:S(2)}, u32[]{:S(2)}) collective-permute-start(bf16[128,128]{0,1:T(8,128)(2,1)S(1)} %get-tuple-element.26), channel_id=1, source_target_pairs={{0,8},{8,16},{16,24},{24,32},{32,40},{40,48},{48,56},{56,64},{64,7... | collective-permute-start | bytes 98312 | tf_op jit(solution)/shard_map/ppermute | solution.py:45
  230.3 161.9 %reduce-scatter.8.cloned.1.call-start = ((), (), s32[]{:S(2)}) async-start(), calls=%async_computation.6 | async-start | bytes 4718592 | tf_op jit(solution)/shard_map/reduce_scatter | solution.py:152
  283.6 1.2 copy-start.3
  284.9 9.8 %collective-permute-start.11 = (bf16[128,2048]{1,0:T(8,128)(2,1)S(1)}, bf16[128,2048]{1,0:T(8,128)(2,1)S(1)}, u32[]{:S(2)}, u32[]{:S(2)}) collective-permute-start(bf16[128,2048]{1,0:T(8,128)(2,1)S(1)} %get-tuple-element.9), channel_id=1, source_target_pairs={{0,1},{1,2},{2,3},{3,4},{4,5},{5,6},{6,7},{7,0},{8,9},{9,10},{10,1... | collective-permute-start | bytes 1572872 | tf_op jit(solution)/shard_map/ppermute | solution.py:21
  284.9 9.8 %collective-permute-start.12 = (bf16[128,2048]{1,0:T(8,128)(2,1)S(1)}, bf16[128,2048]{1,0:T(8,128)(2,1)S(1)}, u32[]{:S(2)}, u32[]{:S(2)}) collective-permute-start(bf16[128,2048]{1,0:T(8,128)(2,1)S(1)} %get-tuple-element.9), channel_id=1, source_target_pairs={{0,7},{1,0},{2,1},{3,2},{4,3},{5,4},{6,5},{7,6},{8,15},{9,8},{10,9... | collective-permute-start | bytes 1572872 | tf_op jit(solution)/shard_map/ppermute | solution.py:24
  294.7 9.8 %collective-permute-start.13 = (bf16[128,2048]{1,0:T(8,128)(2,1)S(1)}, bf16[128,2048]{1,0:T(8,128)(2,1)S(1)}, u32[]{:S(2)}, u32[]{:S(2)}) collective-permute-start(bf16[128,2048]{1,0:T(8,128)(2,1)S(1)} %collective-permute-done.11), channel_id=1, source_target_pairs={{0,1},{1,2},{2,3},{3,4},{4,5},{5,6},{6,7},{7,0},{8,9},{9,10},{10,1... | collective-permute-start | bytes 1572872 | tf_op jit(solution)/shard_map/ppermute | solution.py:21
  294.7 9.9 %collective-permute-start.14 = (bf16[128,2048]{1,0:T(8,128)(2,1)S(1)}, bf16[128,2048]{1,0:T(8,128)(2,1)S(1)}, u32[]{:S(2)}, u32[]{:S(2)}) collective-permute-start(bf16[128,2048]{1,0:T(8,128)(2,1)S(1)} %collective-permute-done.12), channel_id=1, source_target_pairs={{0,7},{1,0},{2,1},{3,2},{4,3},{5,4},{6,5},{7,6},{8,15},{9,8},{10,9... | collective-permute-start | bytes 1572872 | tf_op jit(solution)/shard_map/ppermute | solution.py:24
  304.6 9.8 %collective-permute-start.15 = (bf16[128,2048]{1,0:T(8,128)(2,1)S(1)}, bf16[128,2048]{1,0:T(8,128)(2,1)S(1)}, u32[]{:S(2)}, u32[]{:S(2)}) collective-permute-start(bf16[128,2048]{1,0:T(8,128)(2,1)S(1)} %collective-permute-done.13), channel_id=1, source_target_pairs={{0,1},{1,2},{2,3},{3,4},{4,5},{5,6},{6,7},{7,0},{8,9},{9,10},{10,1... | collective-permute-start | bytes 1572872 | tf_op jit(solution)/shard_map/ppermute | solution.py:21
  304.7 9.8 %collective-permute-start.16 = (bf16[128,2048]{1,0:T(8,128)(2,1)S(1)}, bf16[128,2048]{1,0:T(8,128)(2,1)S(1)}, u32[]{:S(2)}, u32[]{:S(2)}) collective-permute-start(bf16[128,2048]{1,0:T(8,128)(2,1)S(1)} %collective-permute-done.14), channel_id=1, source_target_pairs={{0,7},{1,0},{2,1},{3,2},{4,3},{5,4},{6,5},{7,6},{8,15},{9,8},{10,9... | collective-permute-start | bytes 1572872 | tf_op jit(solution)/shard_map/ppermute | solution.py:24
  314.4 9.8 %collective-permute-start.17 = (bf16[128,2048]{1,0:T(8,128)(2,1)S(1)}, bf16[128,2048]{1,0:T(8,128)(2,1)S(1)}, u32[]{:S(2)}, u32[]{:S(2)}) collective-permute-start(bf16[128,2048]{1,0:T(8,128)(2,1)S(1)} %collective-permute-done.15), channel_id=1, source_target_pairs={{0,1},{1,2},{2,3},{3,4},{4,5},{5,6},{6,7},{7,0},{8,9},{9,10},{10,1... | collective-permute-start | bytes 1572872 | tf_op jit(solution)/shard_map/ppermute | solution.py:21
  331.7 7.6 %collective-permute-start.18 = (bf16[128,128]{0,1:T(8,128)(2,1)S(1)}, bf16[128,128]{0,1:T(8,128)(2,1)S(1)}, u32[]{:S(2)}, u32[]{:S(2)}) collective-permute-start(bf16[128,128]{0,1:T(8,128)(2,1)S(1)} %get-tuple-element.24), channel_id=1, source_target_pairs={{0,8},{8,16},{16,24},{24,32},{32,40},{40,48},{48,56},{56,64},{64,7... | collective-permute-start | bytes 98312 | tf_op jit(solution)/shard_map/ppermute | solution.py:45
  335.1 5.8 %collective-permute-start.19 = (bf16[128,128]{0,1:T(8,128)(2,1)S(1)}, bf16[128,128]{0,1:T(8,128)(2,1)S(1)}, u32[]{:S(2)}, u32[]{:S(2)}) collective-permute-start(bf16[128,128]{0,1:T(8,128)(2,1)S(1)} %get-tuple-element.25), channel_id=1, source_target_pairs={{8,0},{16,8},{24,16},{32,24},{40,32},{48,40},{56,48},{64,56},{72,6... | collective-permute-start | bytes 98312 | tf_op jit(solution)/shard_map/ppermute | solution.py:48
  349.4 44.0 %copy-start.5 = (f32[2048]{0:T(1024)S(1)}, f32[2048]{0:T(1024)}, u32[]{:S(2)}) copy-start(f32[2048]{0:T(1024)} %param.15) | copy-start | bytes 24580
Sparse Core Ops, SparseCore 0:
  10.3 56.4 all-gather.1
  97.1 55.0 reduce-scatter.3
  230.5 53.0 reduce-scatter.5
  353.8 38.3 reduce-scatter.7
